TPU v7x, 512 devices: a whole 4x4x16 slice. The times are simulated.
512 devices in a mesh: dp: 4 (over x), kv: 64 (over z, y), tp: 2 (over core).
Axes of the slice: x: 4, y: 4, z: 16, core: 2. Of those that a mesh axis runs over, the one named last changes fastest.
Arguments:
- tokens: bfloat16 [4, 20480, 2048], P('dp', 'kv'), may hold values from -72 to 72
- w_query: bfloat16 [2048, 512], P(None, 'tp'), may hold values from -0.125 to 0.125
- key_weight: bfloat16 [2048, 256], P(None, 'tp'), may hold values from -0.125 to 0.125
- value_weight: bfloat16 [2048, 256], P(None, 'tp'), may hold values from -2.09375 to 2.09375
- w_out: bfloat16 [512, 2048], P(None, 'tp'), may hold values from -0.25 to 0.25
- chosen: int32 [4, 640, 16], P('dp', 'kv'), may hold values from -1 to 639, as said below
Outputs:
- mixed: bfloat16 [4, 20480, 2048], P('dp', 'kv', 'tp')
- log_mass: float32 [4, 4, 20480], P('dp', 'tp', 'kv')
Inputs may be any that keep to these rules, and one draw needn't show every extreme that they name: `chosen`: entry 0 of row i of a sequence is i; the other entries are distinct blocks before i, or -1 for an empty slot. The 10 rows of one index of kv together name at most one block held by any other index of kv; this bound is reached.
All inputs are finite; a program needn't handle non-finite values.
Results may differ from a plain program's by a relative error of at most 0.006.
The roundings to bfloat16 on the way count: a program that leaves them out, or rounds other values in their place, can miss the bound.
Values may be sent and summed in bfloat16 or wider, within the bound.
A program may use at most 64 MiB of HBM per device.

v0:
```python
import jax
import jax.numpy as jnp
from jax import lax
from jax.sharding import PartitionSpec as P

HEAD_WIDTH = 128


def body(tokens, w_query, key_weight, value_weight, w_out, chosen):
    local_tokens = tokens[0]
    local_chosen = chosen[0]
    row_count = local_tokens.shape[0]
    blocks_here, select_count = local_chosen.shape
    block_rows = row_count // blocks_here
    kv_heads = key_weight.shape[1] // HEAD_WIDTH
    query_heads = w_query.shape[1] // HEAD_WIDTH
    heads_per_group = query_heads // kv_heads
    width_kv = kv_heads * HEAD_WIDTH
    devices = lax.axis_size("kv")
    my_index = lax.axis_index("kv")
    queries = jnp.dot(local_tokens, w_query, preferred_element_type=jnp.float32).astype(
        jnp.bfloat16
    )
    projected_keys = jnp.dot(local_tokens, key_weight, preferred_element_type=jnp.float32).astype(
        jnp.bfloat16
    )
    projected_values = jnp.dot(
        local_tokens, value_weight, preferred_element_type=jnp.float32
    ).astype(jnp.bfloat16)
    paired = jnp.concatenate([projected_keys, projected_values], axis=1)
    owners = local_chosen // blocks_here
    inner_ix = local_chosen % blocks_here
    remote = (local_chosen >= 0) & (owners != my_index)
    peer_ids = jnp.arange(devices, dtype=jnp.int32)
    requests = jnp.where(
        remote[..., None] & (owners[..., None] == peer_ids), inner_ix[..., None], -1
    )
    wanted = jnp.max(requests, axis=(0, 1)).reshape(devices, 1)
    asked_ids = lax.all_to_all(wanted, "kv", split_axis=0, concat_axis=0, tiled=True)
    own_blocks = paired.reshape(blocks_here, block_rows, 2 * width_kv)
    replies = jnp.take(own_blocks, jnp.maximum(asked_ids[:, 0], 0), axis=0)
    arrived = lax.all_to_all(replies, "kv", split_axis=0, concat_axis=0, tiled=True)
    block_table = jnp.concatenate([arrived, own_blocks], axis=0)
    lookup = jnp.where(remote, owners, devices + inner_ix)
    picked = jnp.take(block_table, lookup, axis=0)
    selected_keys = picked[..., :width_kv].reshape(
        blocks_here, select_count * block_rows, kv_heads, HEAD_WIDTH
    )
    selected_values = picked[..., width_kv:].reshape(
        blocks_here, select_count * block_rows, kv_heads, HEAD_WIDTH
    )
    grouped_queries = queries.reshape(
        blocks_here, block_rows, kv_heads, heads_per_group, HEAD_WIDTH
    )
    scores = jnp.einsum(
        "btkgd,bskd->bkgts", grouped_queries, selected_keys, preferred_element_type=jnp.float32
    ) * HEAD_WIDTH ** (-0.5)
    bounded_index = jnp.maximum(local_chosen, 0)
    key_pos = (
        bounded_index[..., None] * block_rows + jnp.arange(block_rows, dtype=jnp.int32)
    ).reshape(blocks_here, select_count * block_rows)
    key_live = jnp.repeat(local_chosen >= 0, block_rows, axis=1)
    block_ids = my_index * blocks_here + jnp.arange(blocks_here, dtype=jnp.int32)
    query_pos = block_ids[:, None] * block_rows + jnp.arange(block_rows, dtype=jnp.int32)[None, :]
    allowed = key_live[:, None, :] & (key_pos[:, None, :] <= query_pos[:, :, None])
    scores = jnp.where(allowed[:, None, None], scores, -jnp.inf)
    row_max = jnp.max(scores, axis=-1)
    weights = jnp.exp(scores - row_max[..., None])
    row_sum = jnp.sum(weights, axis=-1)
    probs_low = weights.astype(jnp.bfloat16)
    summed = jnp.einsum(
        "bkgts,bskd->btkgd", probs_low, selected_values, preferred_element_type=jnp.float32
    )
    attended = (
        (summed / row_sum.transpose(0, 3, 1, 2)[..., None])
        .astype(jnp.bfloat16)
        .reshape(row_count, query_heads * HEAD_WIDTH)
    )
    log_mass = (row_max + jnp.log(row_sum)).transpose(1, 2, 0, 3).reshape(query_heads, row_count)
    mixed = jnp.dot(
        lax.all_gather(attended, "tp", axis=1, tiled=True),
        w_out,
        preferred_element_type=jnp.float32,
    ).astype(jnp.bfloat16)
    return (mixed[None], log_mass[None])


def solution(mesh):
    in_specs = (
        P("dp", "kv", None),
        P(None, "tp"),
        P(None, "tp"),
        P(None, "tp"),
        P(None, "tp"),
        P("dp", "kv", None),
    )
    out_specs = (P("dp", "kv", "tp"), P("dp", "tp", "kv"))
    return jax.shard_map(body, mesh=mesh, in_specs=in_specs, out_specs=out_specs, check_vma=False)
```

profile of v0, /device:TPU:1, one launch (start us, length us, event | category | flops | bytes accessed | tf_op | source)
XLA Modules:
  0.0 116.2 jit_solution(6678006061197199242)
XLA Ops:
  0.6 0.0 copy-start
  0.6 0.0 copy-start.2
  0.7 0.8 broadcast_remainder_fusion
  1.5 0.7 compare_and_fusion.1
  2.2 0.1 select_reduce_fusion
  2.4 0.7 copy.58
  3.1 19.3 %all-to-all-start = ((s32[64,1,1]{2,1,0:T(1,128)}), s32[64,1,1]{2,1,0:T(1,128)S(1)}, u32[]{:S(2)}, u32[]{:S(2)}) async-start(s32[64,1,1]{2,1,0:T(1,128)} %copy.58), calls=%async_computation | async-start | bytes 65536 | tf_op jit(solution)/shard_map/all_to_all | solution.py:39
  22.4 0.0 copy-done
  22.4 1.5 %fusion.14 = bf16[320,128]{1,0:T(8,128)(2,1)S(1)} fusion(bf16[2048,128]{1,0:T(8,128)(2,1)} %param.8, bf16[1,320,2048]{2,1,0:T(8,128)(2,1)S(1)} %copy-done), kind=kOutput, calls=%fused_computation.20 | convolution fusion | flops 167813120 | bytes 1916928 | tf_op jit(solution)/shard_map/dot_general | solution.py:24
  23.9 0.0 copy-done.2
  23.9 0.5 fusion.17
  24.5 11.3 %all-to-all-done = s32[64,1,1]{2,1,0:T(1,128)S(1)} async-done(((s32[64,1,1]{2,1,0:T(1,128)}), s32[64,1,1]{2,1,0:T(1,128)S(1)}, u32[]{:S(2)}, u32[]{:S(2)}) %all-to-all-start) | async-done | bytes 288 | tf_op jit(solution)/shard_map/all_to_all | solution.py:39
  35.8 1.2 %maximum_reduce_fusion = s32[64]{0:T(128)S(1)} fusion(s32[64,1,1]{2,1,0:T(1,128)S(1)} %all-to-all-done), kind=kLoop, calls=%fused_computation.41 | loop fusion | flops 64 | bytes 512 | tf_op jit(solution)/shard_map/max | solution.py:41
  37.0 0.6 gather_fusion
  37.6 1.2 %compare_reduce_fusion = pred[64]{0:T(512)(128)(4,1)S(1)} fusion(s32[64,1,1]{2,1,0:T(1,128)S(1)} %all-to-all-done), kind=kLoop, calls=%fused_computation.31 | loop fusion | flops 128 | bytes 320 | tf_op jit(solution)/shard_map/jit(_take)/le | solution.py:41
  38.9 1.2 %broadcast_select_fusion.1 = bf16[64,32,256]{2,1,0:T(8,128)(2,1)} fusion(bf16[64,32,256]{2,1,0:T(8,128)(2,1)S(1)} %gather_fusion, pred[64]{0:T(512)(128)(4,1)S(1)} %compare_reduce_fusion), kind=kLoop, calls=%fused_computation.24 | loop fusion | flops 524288 | bytes 2097216 | tf_op jit(solution)/shard_map/jit(_take)/select_n | solution.py:41
  40.1 0.0 copy-start.3
  40.1 0.0 copy-start.4
  40.1 5.6 %all-to-all-start.1 = ((bf16[64,32,256]{2,1,0:T(8,128)(2,1)}), bf16[64,32,256]{2,1,0:T(8,128)(2,1)}, u32[]{:S(2)}, u32[]{:S(2)}) async-start(bf16[64,32,256]{2,1,0:T(8,128)(2,1)} %broadcast_select_fusion.1), calls=%async_computation.1 | async-start | bytes 2097152 | tf_op jit(solution)/shard_map/all_to_all | solution.py:42
  45.7 0.0 copy-done.3
  45.8 0.1 fusion.33
  45.9 0.1 reshape.281
  45.9 0.1 broadcast_in_dim.68
  46.0 0.1 and.100
  46.1 0.1 add.151
  46.2 0.1 add.152
  46.3 0.1 add.154
  46.4 0.0 copy-done.4
  46.4 0.5 fusion.9
  47.0 0.1 iota_add_fusion
  47.1 0.2 compare_and_fusion
  47.3 49.6 %all-to-all-done.1 = bf16[64,32,256]{2,1,0:T(8,128)(2,1)} async-done(((bf16[64,32,256]{2,1,0:T(8,128)(2,1)}), bf16[64,32,256]{2,1,0:T(8,128)(2,1)}, u32[]{:S(2)}, u32[]{:S(2)}) %all-to-all-start.1) | async-done | bytes 1048608 | tf_op jit(solution)/shard_map/all_to_all | solution.py:42
  96.9 1.3 %pad_maximum_fusion = bf16[74,32,256]{2,1,0:T(8,128)(2,1)S(1)} fusion(bf16[10,32,256]{2,1,0:T(8,128)(2,1)S(1)} %bitcast.114, bf16[64,32,256]{2,1,0:T(8,128)(2,1)} %all-to-all-done.1), kind=kLoop, calls=%fused_computation.15 | loop fusion | flops 606208 | bytes 2424832 | tf_op jit(solution)/shard_map/concatenate | solution.py:43
  98.3 2.5 %gather_fusion.1 = bf16[160,32,256]{2,1,0:T(8,128)(2,1)} fusion(bf16[74,32,256]{2,1,0:T(8,128)(2,1)S(1)} %pad_maximum_fusion, s32[1024]{0:T(1024)S(1)} %pad_clamp_fusion), kind=kCustom, calls=%fused_computation.1 | custom fusion | bytes 5243520 | tf_op jit(solution)/shard_map/jit(_take)/gather | solution.py:45
  100.8 2.1 %broadcast_select_fusion = bf16[10,16,32,256]{3,2,1,0:T(8,128)(2,1)S(1)} fusion(bf16[10,16,32,256]{3,2,1,0:T(8,128)(2,1)} %bitcast.115, pred[10,16]{1,0:T(8,128)(4,1)S(1)} %get-tuple-element.2), kind=kLoop, calls=%fused_computation.2 | loop fusion | flops 1310720 | bytes 5243040 | tf_op jit(solution)/shard_map/jit(_take)/select_n | solution.py:45
  102.8 1.5 %fusion.37 = (bf16[10,16,32,128]{3,2,1,0:T(8,128)(2,1)S(1)}, bf16[10,16,32,128]{3,2,1,0:T(8,128)(2,1)}) fusion(bf16[10,16,32,256]{3,2,1,0:T(8,128)(2,1)S(1)} %broadcast_select_fusion), kind=kLoop, calls=%fused_computation.71 | loop fusion | bytes 5242880 | tf_op jit(solution)/shard_map/slice | solution.py:46
  104.3 0.7 fusion.38
  105.0 0.5 fusion.12
  105.5 0.7 broadcast_in_dim_reshape.2
  106.2 1.8 %fusion.21 = bf16[10,32,1,2,128]{4,1,3,0,2:T(8,128)(2,1)S(1)} fusion(bf16[10,512,128,1]{2,1,3,0:T(8,128)(2,1)} %bitcast.117, f32[10,1,2,32,512]{4,3,2,0,1:T(8,128)S(1)} %get-tuple-element.11, f32[10,2,32]{2,1,0:T(2,128)S(1)} %get-tuple-element.10, f32[10,32,2]{1,2,0:T(2,128)S(1)} %bitcast.120), kind=kOutput, calls=%fused_computation.23 | convolution fusion | flops 84705280 | bytes 2790400 | tf_op jit(solution)/shard_map/bkgts,bskd->btkgd/dot_general | solution.py:71
  107.9 0.0 copy-start.1
  107.9 0.1 copy.64
  108.1 6.7 %all_gather.3 = bf16[320,512]{1,0:T(8,128)(2,1)S(1)} all-gather(bf16[320,256]{1,0:T(8,128)(2,1)S(1)} %bitcast.119), channel_id=1, replica_groups=mesh['dp'=4,'kv'=64,'tp'=2] {'tp'}, dimensions={1}, use_global_device_ids=true | all-gather | bytes 491520 | tf_op jit(solution)/shard_map/all_gather | solution.py:81
  114.8 0.0 copy-done.1
  114.8 1.3 %fusion.8 = bf16[1,320,1024]{2,1,0:T(8,128)(2,1)} fusion(bf16[320,512]{1,0:T(8,128)(2,1)S(1)} %all_gather.3, bf16[512,1024]{1,0:T(8,128)(2,1)S(1)} %copy-done.1), kind=kOutput, calls=%fused_computation.14 | convolution fusion | flops 335872000 | bytes 2031616 | tf_op jit(solution)/shard_map/dot_general | solution.py:80
  (14 shorter events, 0.2 us)
Async XLA Ops:
  0.6 21.7 %copy-start = (bf16[1,320,2048]{2,1,0:T(8,128)(2,1)S(1)}, bf16[1,320,2048]{2,1,0:T(8,128)(2,1)}, u32[]{:S(2)}) copy-start(bf16[1,320,2048]{2,1,0:T(8,128)(2,1)} %param.6) | copy-start | bytes 3932164
  0.6 23.3 %copy-start.2 = (bf16[2048,128]{1,0:T(8,128)(2,1)S(1)}, bf16[2048,128]{1,0:T(8,128)(2,1)}, u32[]{:S(2)}) copy-start(bf16[2048,128]{1,0:T(8,128)(2,1)} %param.9) | copy-start | bytes 1572868
  3.1 32.7 %all-to-all-start = ((s32[64,1,1]{2,1,0:T(1,128)}), s32[64,1,1]{2,1,0:T(1,128)S(1)}, u32[]{:S(2)}, u32[]{:S(2)}) async-start(s32[64,1,1]{2,1,0:T(1,128)} %copy.58), calls=%async_computation | async-start | bytes 65536 | tf_op jit(solution)/shard_map/all_to_all | solution.py:39
  40.1 5.7 %copy-start.3 = (s32[1,10,16]{2,0,1:T(1,128)S(1)}, s32[1,10,16]{2,0,1:T(1,128)}, u32[]{:S(2)}) copy-start(s32[1,10,16]{2,0,1:T(1,128)} %param.11) | copy-start | bytes 1924
  40.1 6.3 %copy-start.4 = (bf16[2048,256]{1,0:T(8,128)(2,1)S(1)}, bf16[2048,256]{1,0:T(8,128)(2,1)}, u32[]{:S(2)}) copy-start(bf16[2048,256]{1,0:T(8,128)(2,1)} %param.7) | copy-start | bytes 3145732
  40.1 56.9 %all-to-all-start.1 = ((bf16[64,32,256]{2,1,0:T(8,128)(2,1)}), bf16[64,32,256]{2,1,0:T(8,128)(2,1)}, u32[]{:S(2)}, u32[]{:S(2)}) async-start(bf16[64,32,256]{2,1,0:T(8,128)(2,1)} %broadcast_select_fusion.1), calls=%async_computation.1 | async-start | bytes 2097152 | tf_op jit(solution)/shard_map/all_to_all | solution.py:42
  107.9 6.9 %copy-start.1 = (bf16[512,1024]{1,0:T(8,128)(2,1)S(1)}, bf16[512,1024]{1,0:T(8,128)(2,1)}, u32[]{:S(2)}) copy-start(bf16[512,1024]{1,0:T(8,128)(2,1)} %param.10) | copy-start | bytes 3145732
where the time goes:
time: 117 us; the launch traced here: 116 us
  waiting for transfers between devices  60.9 us (52%)
  starting transfers between devices  24.9 us (21%)
  other arithmetic  9.62 us (8%)
  local copies, waits for them, and re-layouts  6.76 us (6%)
  blocking collectives  6.68 us (6%)
  matrix products  6.38 us (5%)
    all_to_all x1, waiting for transfers between devices, body(): lax.all_to_all(replies, 'kv', split_axis=0, concat_axis=0, tiled=True)  49.6 us
    all_to_all x1, starting transfers between devices, body(): lax.all_to_all(wanted, 'kv', split_axis=0, concat_axis=0, tiled=True)  19.3 us
    all_to_all x1, waiting for transfers between devices, body(): lax.all_to_all(wanted, 'kv', split_axis=0, concat_axis=0, tiled=True)  11.3 us
    all_gather x1, blocking collectives, body(): lax.all_gather(attended, 'tp', axis=1, tiled=True)  6.68 us
    all_to_all x1, starting transfers between devices, body(): lax.all_to_all(replies, 'kv', split_axis=0, concat_axis=0, tiled=True)  5.64 us
    gather x1, local copies, waits for them, and re-layouts, body(): picked = jnp.take(block_table, lookup, axis=0)  2.48 us
  transfers between devices with their start and end apart: 2, of which 2 were waited for; matrix products, arithmetic and copies ran while one was open for 3% of the time, Pallas kernels for 0%

commit v1 on v0

v1 whole, which is shorter than its diff:
```python
import functools

import jax
import jax.numpy as jnp
from jax import lax
from jax.experimental import pallas as pl
from jax.experimental.pallas import tpu as pltpu
from jax.sharding import PartitionSpec as P

HEAD_WIDTH = 128
RING_Y = 4
BLOCKS_PER_CHUNK = 2
MASKED = -1e38
LOG2_E = 1.4426950408889634
LN_2 = 0.6931471805599453
SCORE_SCALE = HEAD_WIDTH ** (-0.5) * LOG2_E
MESH = pl.DeviceIdType.MESH
COLUMN_TILE = 128
DEPTH_PARTS = 2
MIX_PARTS = 4
LAG = (9, 2)


def exchange_kernel(
    ring_z,
    blocks_here,
    block_rows,
    tokens_hbm,
    wq_hbm,
    wk_hbm,
    wv_hbm,
    wo_hbm,
    chosen_hbm,
    partner,
    log_out,
    wo,
    own_mixed,
    tok,
    wkv,
    wq,
    kv_sum,
    chosen,
    kvbuf,
    stage,
    table,
    outbox,
    qx,
    m_ref,
    l_ref,
    acc,
    keys_in,
    values_in,
    by_row,
    attended,
    want_all,
    want_smem,
    load_sem,
    part_sem,
    plus_send,
    plus_recv,
    minus_send,
    minus_recv,
    y_send,
    y_recv,
    want_send,
    want_recv,
    tp_send,
    tp_recv,
):
    f32, bf16 = jnp.float32, jnp.bfloat16
    me = lax.axis_index("kv")
    core = lax.axis_index("tp")
    z, y = me // RING_Y, me % RING_Y
    rows = blocks_here * block_rows
    half = ring_z // 2
    wrap_last = half - 2
    chunks = blocks_here // BLOCKS_PER_CHUNK
    up = ((z + 1) % ring_z) * RING_Y + y
    down = ((z + ring_z - 1) % ring_z) * RING_Y + y

    side = [z * RING_Y + (y + d) % RING_Y for d in range(RING_Y)]
    beyond = {
        dz: [((z + dz) % ring_z) * RING_Y + (y + d) % RING_Y for d in range(RING_Y)]
        for dz in (1, ring_z - 1)
    }
    barrier = pltpu.get_barrier_semaphore()
    for peer in [up, down] + side[1:]:
        pl.semaphore_signal(barrier, inc=1, device_id={"kv": peer}, device_id_type=MESH)
    pl.semaphore_signal(barrier, inc=1, device_id={"tp": 1 - core}, device_id_type=MESH)

    part_depth = tok.shape[1] // DEPTH_PARTS

    def loads_of(i):
        deep = pl.ds(pl.multiple_of(i * part_depth, part_depth), part_depth)
        k_lanes, v_lanes = pl.ds(0, HEAD_WIDTH), pl.ds(HEAD_WIDTH, HEAD_WIDTH)
        return [
            pltpu.make_async_copy(tokens_hbm.at[0, :, deep], tok.at[:, deep], part_sem.at[i, 0]),
            pltpu.make_async_copy(wk_hbm.at[deep], wkv.at[deep, k_lanes], part_sem.at[i, 1]),
            pltpu.make_async_copy(wv_hbm.at[deep], wkv.at[deep, v_lanes], part_sem.at[i, 2]),
        ]

    load_chosen = pltpu.make_async_copy(chosen_hbm, chosen, load_sem.at[0])
    load_wq = pltpu.make_async_copy(wq_hbm, wq, load_sem.at[1])
    load_wo = pltpu.make_async_copy(wo_hbm, wo, load_sem.at[2])
    load_chosen.start()
    for i in range(DEPTH_PARTS):
        for load in loads_of(i):
            load.start()

    with jax.named_scope("project_kv"):
        kv_sum[...] = jnp.zeros_like(kv_sum)

        @pl.loop(0, DEPTH_PARTS)
        def _(i):
            for load in loads_of(i):
                load.wait()
            deep = pl.ds(pl.multiple_of(i * part_depth, part_depth), part_depth)
            kv_sum[...] += jnp.dot(tok[:, deep], wkv[deep, :], preferred_element_type=f32)

        load_wq.start()
        load_wo.start()
        own = kv_sum[...].astype(bf16)
        for i in range(blocks_here):
            kvbuf[0, i] = own[i * block_rows : (i + 1) * block_rows, :]

    with jax.named_scope("barrier"):
        pl.semaphore_wait(barrier, RING_Y + 2)

    def ring_copy(going_up, src_slot, dst_slot, c):
        view = pl.ds(c * BLOCKS_PER_CHUNK, BLOCKS_PER_CHUNK)
        step = dst_slot if going_up else ring_z - dst_slot
        return pltpu.make_async_remote_copy(
            src_ref=kvbuf.at[src_slot, view],
            dst_ref=kvbuf.at[dst_slot, view],
            send_sem=(plus_send if going_up else minus_send).at[0],
            recv_sem=(plus_recv if going_up else minus_recv).at[step - 1, c],
            device_id={"kv": up if going_up else down},
            device_id_type=MESH,
        )

    def sent(ref, sem, count):
        view = ref.at[pl.ds(0, count)]
        pltpu.make_async_remote_copy(
            src_ref=view,
            dst_ref=view,
            send_sem=sem,
            recv_sem=plus_recv.at[0, 0],
            device_id={"kv": up},
            device_id_type=MESH,
        ).wait_send()

    last_up, last_down = half - 2, half - 1

    def from_below(t):
        return (z >= t) & (t <= last_up)

    def to_above(t):
        return (z >= t) & (z < ring_z - 1) & (t < last_up)

    def from_above(t):
        return ((z + t) % ring_z <= last_down) & (t <= last_down)

    def to_below(t):
        source = (z + t) % ring_z
        return (source <= last_down) & (t < last_down)

    chosen_up = (z >= last_up) & (z < ring_z - 1)
    chosen_down = (z + last_down) % ring_z <= last_down

    with jax.named_scope("first_sends"):
        for c in range(chunks):

            @pl.when(to_above(0))
            def _():
                ring_copy(True, 0, 1, c).start()

            @pl.when(to_below(0))
            def _():
                ring_copy(False, 0, ring_z - 1, c).start()

    lanes = RING_Y * ring_z
    load_chosen.wait()
    lane = lax.broadcasted_iota(jnp.int32, (blocks_here, 128), 1)
    back_y, back_z = lane // ring_z, lane % ring_z
    source = ((z - back_z + ring_z) % ring_z) * RING_Y + (y - back_y + RING_Y) % RING_Y
    low = jnp.where(lane < lanes, source * blocks_here, me * blocks_here + lane - lanes)
    width = jnp.where(
        lane == 0,
        0,
        jnp.where(lane < lanes, blocks_here, jnp.where(lane < lanes + blocks_here, 1, 0)),
    )
    best = jnp.full((blocks_here, 128), -1, jnp.int32)
    picks = chosen[...].reshape(blocks_here, chosen.shape[2])
    for slot in range(chosen.shape[2]):
        inner = picks[:, slot : slot + 1] - low
        best = jnp.where((inner >= 0) & (inner < width), inner, best)
    mask_rows = jnp.where(best >= 0, 0.0, MASKED).astype(f32)
    want = jnp.maximum(best[0:1, :], 0)
    for i in range(1, blocks_here):
        want = jnp.maximum(want, best[i : i + 1, :])
    want_all[0] = want
    def want_copy(source, target, sem, peer):
        return pltpu.make_async_remote_copy(
            src_ref=want_all.at[source],
            dst_ref=want_all.at[target],
            send_sem=want_send.at[sem],
            recv_sem=want_recv.at[sem],
            device_id={"kv": peer},
            device_id_type=MESH,
        )

    row = pl.ds(0, RING_Y)
    rest = pl.ds(1, RING_Y - 1)
    want_side = want_copy(rest, rest, 0, up)
    want_up = want_copy(row, pl.ds(2 * RING_Y, RING_Y), 1, up)
    want_down = want_copy(row, pl.ds(RING_Y, RING_Y), 2, down)
    for d in (2, 1, 3):
        want_copy(0, RING_Y - d, 0, side[d]).start()

    for head in range(qx.shape[0] // rows):
        for i in range(blocks_here):
            qx[pl.ds(head * rows + i * block_rows, block_rows), HEAD_WIDTH:] = jnp.broadcast_to(
                mask_rows[i : i + 1, :], (block_rows, 128)
            ).astype(bf16)

    for slot in range(1, ring_z):

        @pl.when(z < slot)
        def _():
            table[slot] = jnp.zeros(table.shape[1:], bf16)

    with jax.named_scope("project_q"):
        load_wq.wait()
        queries = jnp.dot(tok[...], wq[...], preferred_element_type=f32).astype(bf16)
        heads = qx.shape[0] // rows
        for head in range(heads):
            qx[pl.ds(head * rows, rows), 0:HEAD_WIDTH] = queries[
                :, head * HEAD_WIDTH : (head + 1) * HEAD_WIDTH
            ]

    columns = qx.shape[0]
    tiles = columns // COLUMN_TILE

    def attend(tile, count, first):
        begin, size = (0, columns) if tile is None else (tile * COLUMN_TILE, COLUMN_TILE)
        here = pl.ds(begin, size)
        s = lax.dot_general(
            keys_in[0:count, :],
            qx[here, :],
            (((1,), (1,)), ((), ())),
            preferred_element_type=f32,
        ) * SCORE_SCALE
        if first:
            row = lax.broadcasted_iota(jnp.int32, s.shape, 1) + begin
            row = jnp.where(row >= rows, row - rows, row)
            s = jnp.where(lax.broadcasted_iota(jnp.int32, s.shape, 0) <= row, s, MASKED)
        top = jnp.max(s, axis=0, keepdims=True)
        if first:
            new_m = top
        else:
            old_m = m_ref[:, here]
            new_m = jnp.maximum(old_m, top)
            shrink = jnp.exp2(old_m - new_m)
        p = jnp.exp2(s - new_m)
        total = jnp.sum(p, axis=0, keepdims=True)
        summed = jnp.dot(values_in[:, 0:count], p.astype(bf16), preferred_element_type=f32)
        m_ref[:, here] = new_m
        if first:
            l_ref[:, here] = total
            acc[:, here] = summed
        else:
            l_ref[:, here] = l_ref[:, here] * shrink + total
            acc[:, here] = acc[:, here] * shrink + summed

    def attend_own():
        key_lane = lax.broadcasted_iota(jnp.int32, (rows, 128), 1)
        key_block = lax.broadcasted_iota(jnp.int32, (rows, 128), 0) // block_rows
        own_hot = jnp.where(key_lane == key_block + lanes, 1.0, 0.0).astype(bf16)
        own = kvbuf[0].reshape(rows, 2 * HEAD_WIDTH)
        keys_in[0:rows, 0:HEAD_WIDTH] = own[:, 0:HEAD_WIDTH]
        keys_in[0:rows, HEAD_WIDTH:] = own_hot
        values_in[:, 0:rows] = own[:, HEAD_WIDTH:].T
        attend(None, rows, True)

    def arrival(slot):
        return y_recv.at[jnp.where(slot > half + 1, ring_z - slot, slot)]

    def chosen_copy(d, slot, peer, kind):
        return pltpu.make_async_remote_copy(
            src_ref=outbox.at[slot, d],
            dst_ref=table.at[slot, d],
            send_sem=y_send.at[kind],
            recv_sem=arrival(slot),
            device_id={"kv": peer},
            device_id_type=MESH,
        )

    def arrived(slot, count, first):
        view = table.at[pl.ds(0, count), pl.ds(first, RING_Y - first)]
        pltpu.make_async_remote_copy(
            src_ref=view,
            dst_ref=view,
            send_sem=y_send.at[0],
            recv_sem=arrival(slot),
            device_id={"kv": up},
            device_id_type=MESH,
        ).wait_recv()

    def pass_on(slot):
        stage[...] = kvbuf[slot]
        for d in (2, 1, 3):
            outbox[slot, d] = stage[want_smem[d, 0, d * ring_z + slot]]
            chosen_copy(d, slot, side[d], 0).start()
        table[slot, 0] = stage[want_smem[0, 0, slot]]

    def pass_beyond(dz, held, slot):
        stage[...] = kvbuf[held]
        for d in (2, 1, 3, 0):
            row_there = (RING_Y if dz == 1 else 2 * RING_Y) + d
            outbox[slot, d] = stage[want_smem[row_there, 0, d * ring_z + slot]]
            chosen_copy(d, slot, beyond[dz][d], 1 if dz == 1 else 2).start()

    near_keys = RING_Y * block_rows

    def attend_slots(tile, slots):
        if not tile:
            lane_row = lax.broadcasted_iota(jnp.int32, (near_keys, 128), 1)
            back = lax.broadcasted_iota(jnp.int32, (near_keys, 128), 0) // block_rows * ring_z
            for i, slot in enumerate(slots):
                both = table[slot].reshape(near_keys, 2 * HEAD_WIDTH)
                here = slice(i * near_keys, (i + 1) * near_keys)
                keys_in[here, 0:HEAD_WIDTH] = both[:, 0:HEAD_WIDTH]
                keys_in[here, HEAD_WIDTH:] = jnp.where(
                    lane_row == back + slot, 1.0, 0.0
                ).astype(bf16)
                values_in[:, here] = both[:, HEAD_WIDTH:].T
        attend(tile, len(slots) * near_keys, False)

    def due_from_above(t, c):
        behind = (t - 1) * chunks + c - (LAG[0] * (ring_z - 1 - z)) // LAG[1]
        m = jnp.maximum(behind, 0)
        crossed = z > last_down
        hops = jnp.where(crossed, m // chunks + ring_z - z, t)
        chunk = jnp.where(crossed, m % chunks, c)
        due = jnp.where(crossed, (behind >= 0) & (hops <= last_down), from_above(t))
        return due, hops, chunk

    def step(t, fill):
        for c in range(chunks):

            @pl.when(from_below(t))
            def _():
                ring_copy(True, t, t, c).wait_recv()

            @pl.when(to_above(t))
            def _():
                ring_copy(True, t, t + 1, c).start()

            due, hops, chunk = due_from_above(t, c)
            back = ring_z - hops

            @pl.when(due)
            def _():
                ring_copy(False, back, back, chunk).wait_recv()

            @pl.when(due & (hops < last_down))
            def _():
                ring_copy(False, back, back - 1, chunk).start()

            @pl.when(due & (chunk == chunks - 1) & (hops == last_down) & chosen_down)
            def _():
                pass_beyond(ring_z - 1, ring_z - last_down, half)

            @pl.when(due & (chunk == chunks - 1) & (z >= back))
            def _():
                pass_on(back)

            if c < chunks - 1:
                fill(c)

        if t is last_up:

            @pl.when(chosen_up)
            def _():
                pass_beyond(1, last_up, last_up + 1)

        if t is not last_down:

            @pl.when(z >= t)
            def _():
                pass_on(t)

        fill(chunks - 1)

    def near_slots(t):
        @pl.when((z >= t) & (z < ring_z - t))
        def _():
            arrived(t, 1, 1)

        @pl.when(z >= ring_z - t)
        def _():
            arrived(t, 2, 1)

    near_scalars = pltpu.make_async_copy(want_all.at[row], want_smem.at[row], load_sem.at[3])
    far_rows = pl.ds(RING_Y, 2 * RING_Y)
    far_scalars = pltpu.make_async_copy(want_all.at[far_rows], want_smem.at[far_rows], load_sem.at[3])

    def fill_first(c):
        if c == 1:
            want_side.wait()
            want_up.start()
            want_down.start()
            near_scalars.start()
        if c == chunks - 2:
            near_scalars.wait()
            pass_on(0)

    def fill_second(c):
        if c == chunks - 1:
            want_up.wait()
            want_down.wait()
            far_scalars.start()
            arrived(0, 1, 1)
            attend_slots(None, [0])
            far_scalars.wait()

    def fill_near(t, c):
        if c == 1:
            near_slots(t)
        for tile in {0: [], 1: [0], 2: [1, 2], 3: [3], 4: [4]}[c]:

            @pl.when(z >= t)
            def _():
                attend_slots(tile, [t, ring_z - t])

    share = pltpu.make_async_remote_copy(
        src_ref=attended,
        dst_ref=partner,
        send_sem=tp_send,
        recv_sem=tp_recv,
        device_id={"tp": 1 - core},
        device_id_type=MESH,
    )

    def finish():
        with jax.named_scope("normalise"):
            for tile in range(tiles):
                here = slice(tile * COLUMN_TILE, (tile + 1) * COLUMN_TILE)
                by_row[here, :] = (acc[:, here] / l_ref[:, here]).T.astype(bf16)
            for h in range(heads):
                attended[:, h * HEAD_WIDTH : (h + 1) * HEAD_WIDTH] = by_row[
                    h * rows : (h + 1) * rows, :
                ]
            share.start()
            load_wo.wait()
            width = heads * HEAD_WIDTH
            mine = pl.ds(pl.multiple_of(core * width, width), width)
            own_mixed[...] = jnp.dot(attended[...], wo[mine, :], preferred_element_type=f32)

        mass = m_ref[...] * LN_2 + jnp.log(l_ref[...])
        for h in range(heads):
            log_out[0, h : h + 1, :] = mass[:, h * rows : (h + 1) * rows]

    with jax.named_scope("own"):
        attend_own()
    with jax.named_scope("step_1"):
        step(1, fill_first)
    with jax.named_scope("step_2"):
        step(2, fill_second)

    @pl.loop(3, last_up)
    def _(t):
        with jax.named_scope("step_t"):
            step(t, functools.partial(fill_near, t - 2))

    @pl.when(z == 0)
    def _():
        finish()

    with jax.named_scope("step_6"):
        step(last_up, functools.partial(fill_near, last_up - 2))
    with jax.named_scope("step_7"):
        step(last_down, functools.partial(fill_near, last_down - 2))

    with jax.named_scope("last_but_one"):
        near_slots(last_up)

        @pl.when(z > last_up)
        def _():
            arrived(last_up + 1, 1, 0)

        @pl.when(z >= last_up)
        def _():
            attend_slots(None, [last_up, ring_z - last_up, last_up + 1])

    with jax.named_scope("last_wait"):

        @pl.when(z >= half)
        def _():
            arrived(half, 1, 0)

        @pl.when(z > half)
        def _():
            arrived(half + 1, 1, 1)

    with jax.named_scope("last"):

        @pl.when(z >= half)
        def _():
            attend_slots(None, [half, half + 1])

    @pl.when(z > 0)
    def _():
        finish()

    with jax.named_scope("sends"):
        ups = jnp.where(z < ring_z - 1, jnp.minimum(z + 1, last_up), 0)
        for n in range(1, last_up + 1):

            @pl.when(ups == n)
            def _():
                sent(kvbuf, plus_send.at[0], n)

        downs = jnp.where(
            z <= last_down,
            jnp.minimum(last_down + 1 - z, last_down),
            jnp.maximum(z - (ring_z - last_down), 0),
        )
        for n in range(1, last_down + 1):

            @pl.when(downs == n)
            def _():
                sent(kvbuf, minus_send.at[0], n)

        passes = jnp.minimum(z, last_up) + jnp.maximum(z - (ring_z - last_down - 1), 0) + 1
        for n in range(1, last_up + last_down + 2):

            @pl.when(passes == n)
            def _():
                sent(outbox.at[:, pl.ds(1, RING_Y - 1)], y_send.at[0], n)

        @pl.when(chosen_up)
        def _():
            sent(outbox, y_send.at[1], 1)

        @pl.when(chosen_down)
        def _():
            sent(outbox, y_send.at[2], 1)

    share.wait()


def mix_kernel(partner, wo, own_mixed, log_in, mixed_hbm, log_hbm, mixed, log_vmem, sem):
    width = partner.shape[1]
    other = 1 - lax.axis_index("tp")
    theirs = pl.ds(pl.multiple_of(other * width, width), width)
    log_vmem[...] = log_in[...]
    copies = [pltpu.make_async_copy(log_vmem, log_hbm, sem.at[0])]
    copies[0].start()
    step = wo.shape[1] // MIX_PARTS
    for i in range(MIX_PARTS):
        here = slice(i * step, (i + 1) * step)
        mixed[0, :, here] = (
            own_mixed[:, here]
            + jnp.dot(partner[...], wo[theirs, here], preferred_element_type=jnp.float32)
        ).astype(jnp.bfloat16)
        copy = pltpu.make_async_copy(
            mixed.at[:, :, pl.ds(i * step, step)], mixed_hbm.at[:, :, pl.ds(i * step, step)], sem.at[i + 1]
        )
        copy.start()
        copies.append(copy)
    for copy in copies:
        copy.wait()


def body(tokens, w_query, key_weight, value_weight, w_out, chosen):
    row_count, depth = tokens.shape[1], tokens.shape[2]
    blocks_here, slots = chosen.shape[1:]
    block_rows = row_count // blocks_here
    ring_z = lax.axis_size("kv") // RING_Y
    q_width = w_query.shape[1]
    heads = q_width // HEAD_WIDTH
    kv_width = key_weight.shape[1] + value_weight.shape[1]
    chunks = blocks_here // BLOCKS_PER_CHUNK
    dma = pltpu.SemaphoreType.DMA
    vmem = pltpu.VMEM
    hbm = lambda x: pltpu.with_memory_space_constraint(x, pltpu.HBM)
    partner, log_part, wo, own_mixed = pl.pallas_call(
        functools.partial(exchange_kernel, ring_z, blocks_here, block_rows),
        out_shape=(
            vmem((row_count, q_width), jnp.bfloat16),
            vmem((1, heads, row_count), jnp.float32),
            vmem(w_out.shape, jnp.bfloat16),
            vmem((row_count, w_out.shape[1]), jnp.float32),
        ),
        in_specs=[pl.BlockSpec(memory_space=pl.ANY)] * 6,
        out_specs=(pl.BlockSpec(memory_space=vmem),) * 4,
        scratch_shapes=[
            vmem((row_count, depth), jnp.bfloat16),
            vmem((depth, kv_width), jnp.bfloat16),
            vmem((depth, q_width), jnp.bfloat16),
            vmem((row_count, kv_width), jnp.float32),
            vmem((blocks_here, 1, slots), jnp.int32),
            vmem((ring_z, blocks_here, block_rows, kv_width), jnp.bfloat16),
            vmem((blocks_here, block_rows, kv_width), jnp.bfloat16),
            vmem((ring_z, RING_Y, block_rows, kv_width), jnp.bfloat16),
            vmem((ring_z, RING_Y, block_rows, kv_width), jnp.bfloat16),
            vmem((heads * row_count, 2 * HEAD_WIDTH), jnp.bfloat16),
            vmem((1, heads * row_count), jnp.float32),
            vmem((1, heads * row_count), jnp.float32),
            vmem((HEAD_WIDTH, heads * row_count), jnp.float32),
            vmem((max(row_count, 3 * RING_Y * block_rows), 2 * HEAD_WIDTH), jnp.bfloat16),
            vmem((HEAD_WIDTH, max(row_count, 3 * RING_Y * block_rows)), jnp.bfloat16),
            vmem((heads * row_count, HEAD_WIDTH), jnp.bfloat16),
            vmem((row_count, q_width), jnp.bfloat16),
            vmem((3 * RING_Y, 1, 128), jnp.int32),
            pltpu.SMEM((3 * RING_Y, 1, 128), jnp.int32),
            dma((4,)),
            dma((DEPTH_PARTS, 3)),
            dma((1,)),
            dma((ring_z // 2 - 2, chunks)),
            dma((1,)),
            dma((ring_z // 2 - 1, chunks)),
            dma((3,)),
            dma((ring_z // 2 + 2,)),
            dma((3,)),
            dma((3,)),
            dma,
            dma,
        ],
        compiler_params=pltpu.CompilerParams(
            collective_id=0, has_side_effects=True, vmem_limit_bytes=40 * 1024 * 1024
        ),
    )(*map(hbm, (tokens, w_query, key_weight, value_weight, w_out, chosen.reshape(blocks_here, 1, slots))))
    return pl.pallas_call(
        mix_kernel,
        out_shape=(
            jax.ShapeDtypeStruct((1, row_count, w_out.shape[1]), jnp.bfloat16),
            jax.ShapeDtypeStruct((1, heads, row_count), jnp.float32),
        ),
        in_specs=[pl.BlockSpec(memory_space=vmem)] * 4,
        out_specs=(pl.BlockSpec(memory_space=pl.ANY),) * 2,
        scratch_shapes=[
            vmem((1, row_count, w_out.shape[1]), jnp.bfloat16),
            vmem((1, heads, row_count), jnp.float32),
            dma((MIX_PARTS + 1,)),
        ],
        compiler_params=pltpu.CompilerParams(vmem_limit_bytes=12 * 1024 * 1024),
    )(partner, wo, own_mixed, log_part)


def solution(mesh):
    in_specs = (
        P("dp", "kv", None),
        P(None, "tp"),
        P(None, "tp"),
        P(None, "tp"),
        P(None, "tp"),
        P("dp", "kv", None),
    )
    out_specs = (P("dp", "kv", "tp"), P("dp", "tp", "kv"))
    return jax.shard_map(body, mesh=mesh, in_specs=in_specs, out_specs=out_specs, check_vma=False)
```

time: 117 us -> 40.4 us (0.35)
  the two profiles are of different devices: /device:TPU:1 before, /device:TPU:12 now
where the time goes in v1:
time: 40.4 us; the launch traced here: 40.3 us
  Pallas kernels  39.6 us (98%)
  between operations  0.64 us (2%)
    pallas_call x1, Pallas kernels, body(): pl.pallas_call(functools.partial(exchange_kernel, ring_z, blocks_here, bl...  38.5 us
    pallas_call x1, Pallas kernels, body(): pl.pallas_call(mix_kernel, out_shape=(jax.ShapeDtypeStruct((1, row_count,...  1.15 us

profile of v1, /device:TPU:12, one launch (start us, length us, event | category | flops | bytes accessed | tf_op | source)
XLA Modules:
  0.0 40.3 jit_solution(983863247329114880)
XLA Ops:
  0.6 38.5 %shard_map.77 = (bf16[320,256]{1,0:T(8,128)(2,1)S(1)}, f32[1,2,320]{2,1,0:T(2,128)S(1)}, bf16[512,1024]{1,0:T(8,128)(2,1)S(1)}, f32[320,1024]{1,0:T(8,128)S(1)}) custom-call(bf16[1,320,2048]{2,1,0:T(8,128)(2,1)} %tokens_hbm.1, bf16[2048,256]{1,0:T(8,128)(2,1)} %wq_hbm.1, bf16[2048,128]{1,0:T(8,128)(2,1)} %wk_hbm.1, bf16[2048,128]{1,0:T(8,128)(2,1)} %wv_hbm.1, ...), custom_call_target="tpu_custom_call" | custom-call | tf_op jit(solution)/shard_map/pallas_call | solution.py:588
  39.1 1.1 %shard_map.78 = (bf16[1,320,1024]{2,1,0:T(8,128)(2,1)}, f32[1,2,320]{2,1,0:T(2,128)}) custom-call(bf16[320,256]{1,0:T(8,128)(2,1)S(1)} %get-tuple-element.6.partner, bf16[512,1024]{1,0:T(8,128)(2,1)S(1)} %get-tuple-element.7.wo, f32[320,1024]{1,0:T(8,128)S(1)} %get-tuple-element.8.own_mixed, f32[1,2,320]{2,1,0:T(2,128)S(1)} %get-tuple-element.9.log_in), custom_call_target="tpu_custom_call" | custom-call | tf_op jit(solution)/shard_map/pallas_call | solution.py:635

commit v2 on v1

--- a/solution.py
+++ b/solution.py
@@ -84,10 +84,6 @@
         for dz in (1, ring_z - 1)
     }
     barrier = pltpu.get_barrier_semaphore()
-    for peer in [up, down] + side[1:]:
-        pl.semaphore_signal(barrier, inc=1, device_id={"kv": peer}, device_id_type=MESH)
-    pl.semaphore_signal(barrier, inc=1, device_id={"tp": 1 - core}, device_id_type=MESH)
-
     part_depth = tok.shape[1] // DEPTH_PARTS
 
     def loads_of(i):
@@ -102,10 +98,14 @@
     load_chosen = pltpu.make_async_copy(chosen_hbm, chosen, load_sem.at[0])
     load_wq = pltpu.make_async_copy(wq_hbm, wq, load_sem.at[1])
     load_wo = pltpu.make_async_copy(wo_hbm, wo, load_sem.at[2])
-    load_chosen.start()
     for i in range(DEPTH_PARTS):
         for load in loads_of(i):
             load.start()
+    load_chosen.start()
+    for peer in [up, down] + side[1:]:
+        pl.semaphore_signal(barrier, inc=1, device_id={"kv": peer}, device_id_type=MESH)
+    pl.semaphore_signal(barrier, inc=1, device_id={"tp": 1 - core}, device_id_type=MESH)
+
 
     with jax.named_scope("project_kv"):
         kv_sum[...] = jnp.zeros_like(kv_sum)
@@ -310,14 +310,16 @@
         stage[...] = kvbuf[slot]
         for d in (2, 1, 3):
             outbox[slot, d] = stage[want_smem[d, 0, d * ring_z + slot]]
+        table[slot, 0] = stage[want_smem[0, 0, slot]]
+        for d in (2, 1, 3):
             chosen_copy(d, slot, side[d], 0).start()
-        table[slot, 0] = stage[want_smem[0, 0, slot]]
 
     def pass_beyond(dz, held, slot):
         stage[...] = kvbuf[held]
         for d in (2, 1, 3, 0):
             row_there = (RING_Y if dz == 1 else 2 * RING_Y) + d
             outbox[slot, d] = stage[want_smem[row_there, 0, d * ring_z + slot]]
+        for d in (2, 1, 3, 0):
             chosen_copy(d, slot, beyond[dz][d], 1 if dz == 1 else 2).start()
 
     near_keys = RING_Y * block_rows
@@ -451,8 +453,8 @@
                 attended[:, h * HEAD_WIDTH : (h + 1) * HEAD_WIDTH] = by_row[
                     h * rows : (h + 1) * rows, :
                 ]
+            load_wo.wait()
             share.start()
-            load_wo.wait()
             width = heads * HEAD_WIDTH
             mine = pl.ds(pl.multiple_of(core * width, width), width)
             own_mixed[...] = jnp.dot(attended[...], wo[mine, :], preferred_element_type=f32)

time: 40.4 us -> 40.4 us (level)
  the two profiles are of different devices: /device:TPU:12 before, /device:TPU:8 now
where the time goes in v2:
time: 40.4 us; the launch traced here: 40.3 us
  Pallas kernels  39.6 us (98%)
  between operations  0.64 us (2%)
    pallas_call x1, Pallas kernels, body(): pl.pallas_call(functools.partial(exchange_kernel, ring_z, blocks_here, bl...  38.5 us
    pallas_call x1, Pallas kernels, body(): pl.pallas_call(mix_kernel, out_shape=(jax.ShapeDtypeStruct((1, row_count,...  1.15 us

profile of v2, /device:TPU:8, one launch (start us, length us, event | category | flops | bytes accessed | tf_op | source)
XLA Modules:
  0.0 40.3 jit_solution(7224097755094390478)
XLA Ops:
  0.6 38.5 %shard_map.77 = (bf16[320,256]{1,0:T(8,128)(2,1)S(1)}, f32[1,2,320]{2,1,0:T(2,128)S(1)}, bf16[512,1024]{1,0:T(8,128)(2,1)S(1)}, f32[320,1024]{1,0:T(8,128)S(1)}) custom-call(bf16[1,320,2048]{2,1,0:T(8,128)(2,1)} %tokens_hbm.1, bf16[2048,256]{1,0:T(8,128)(2,1)} %wq_hbm.1, bf16[2048,128]{1,0:T(8,128)(2,1)} %wk_hbm.1, bf16[2048,128]{1,0:T(8,128)(2,1)} %wv_hbm.1, ...), custom_call_target="tpu_custom_call" | custom-call | tf_op jit(solution)/shard_map/pallas_call | solution.py:590
  39.1 1.1 %shard_map.78 = (bf16[1,320,1024]{2,1,0:T(8,128)(2,1)}, f32[1,2,320]{2,1,0:T(2,128)}) custom-call(bf16[320,256]{1,0:T(8,128)(2,1)S(1)} %get-tuple-element.6.partner, bf16[512,1024]{1,0:T(8,128)(2,1)S(1)} %get-tuple-element.7.wo, f32[320,1024]{1,0:T(8,128)S(1)} %get-tuple-element.8.own_mixed, f32[1,2,320]{2,1,0:T(2,128)S(1)} %get-tuple-element.9.log_in), custom_call_target="tpu_custom_call" | custom-call | tf_op jit(solution)/shard_map/pallas_call | solution.py:637

commit v3 on v2

--- a/solution.py
+++ b/solution.py
@@ -126,6 +126,20 @@
     with jax.named_scope("barrier"):
         pl.semaphore_wait(barrier, RING_Y + 2)
 
+    def ring_arrival(going_up, step, c):
+        sems, last_hop = (plus_recv, last_up) if going_up else (minus_recv, last_down)
+        return sems.at[jnp.minimum((step - 1) * chunks + c, (last_hop - 1) * chunks)]
+
+    def whole_slot(going_up, slot, step):
+        return pltpu.make_async_remote_copy(
+            src_ref=kvbuf.at[slot],
+            dst_ref=kvbuf.at[slot],
+            send_sem=(plus_send if going_up else minus_send).at[0],
+            recv_sem=ring_arrival(going_up, step, 0),
+            device_id={"kv": up},
+            device_id_type=MESH,
+        )
+
     def ring_copy(going_up, src_slot, dst_slot, c):
         view = pl.ds(c * BLOCKS_PER_CHUNK, BLOCKS_PER_CHUNK)
         step = dst_slot if going_up else ring_z - dst_slot
@@ -133,7 +147,7 @@
             src_ref=kvbuf.at[src_slot, view],
             dst_ref=kvbuf.at[dst_slot, view],
             send_sem=(plus_send if going_up else minus_send).at[0],
-            recv_sem=(plus_recv if going_up else minus_recv).at[step - 1, c],
+            recv_sem=ring_arrival(going_up, step, c),
             device_id={"kv": up if going_up else down},
             device_id_type=MESH,
         )
@@ -144,7 +158,7 @@
             src_ref=view,
             dst_ref=view,
             send_sem=sem,
-            recv_sem=plus_recv.at[0, 0],
+            recv_sem=plus_recv.at[0],
             device_id={"kv": up},
             device_id_type=MESH,
         ).wait_send()
@@ -242,7 +256,7 @@
     tiles = columns // COLUMN_TILE
 
     def attend(tile, count, first):
-        begin, size = (0, columns) if tile is None else (tile * COLUMN_TILE, COLUMN_TILE)
+        begin, size = (0, columns) if tile is None else tile
         here = pl.ds(begin, size)
         s = lax.dot_general(
             keys_in[0:count, :],
@@ -325,7 +339,7 @@
     near_keys = RING_Y * block_rows
 
     def attend_slots(tile, slots):
-        if not tile:
+        if tile is None or tile[0] == 0:
             lane_row = lax.broadcasted_iota(jnp.int32, (near_keys, 128), 1)
             back = lax.broadcasted_iota(jnp.int32, (near_keys, 128), 0) // block_rows * ring_z
             for i, slot in enumerate(slots):
@@ -350,9 +364,17 @@
     def step(t, fill):
         for c in range(chunks):
 
-            @pl.when(from_below(t))
-            def _():
-                ring_copy(True, t, t, c).wait_recv()
+            if t is not last_up:
+
+                @pl.when(from_below(t))
+                def _():
+                    ring_copy(True, t, t, c).wait_recv()
+
+            elif c == chunks - 1:
+
+                @pl.when(from_below(t))
+                def _():
+                    whole_slot(True, t, t).wait_recv()
 
             @pl.when(to_above(t))
             def _():
@@ -361,9 +383,13 @@
             due, hops, chunk = due_from_above(t, c)
             back = ring_z - hops
 
-            @pl.when(due)
+            @pl.when(due & (hops < last_down))
             def _():
                 ring_copy(False, back, back, chunk).wait_recv()
+
+            @pl.when(due & (hops == last_down) & (chunk == chunks - 1))
+            def _():
+                whole_slot(False, ring_z - last_down, last_down).wait_recv()
 
             @pl.when(due & (hops < last_down))
             def _():
@@ -429,7 +455,8 @@
     def fill_near(t, c):
         if c == 1:
             near_slots(t)
-        for tile in {0: [], 1: [0], 2: [1, 2], 3: [3], 4: [4]}[c]:
+        wide = 3 * COLUMN_TILE
+        for tile in {1: [(0, wide)], 3: [(wide, columns - wide)]}.get(c, []):
 
             @pl.when(z >= t)
             def _():
@@ -620,9 +647,9 @@
             dma((4,)),
             dma((DEPTH_PARTS, 3)),
             dma((1,)),
-            dma((ring_z // 2 - 2, chunks)),
+            dma(((ring_z // 2 - 3) * chunks + 1,)),
             dma((1,)),
-            dma((ring_z // 2 - 1, chunks)),
+            dma(((ring_z // 2 - 2) * chunks + 1,)),
             dma((3,)),
             dma((ring_z // 2 + 2,)),
             dma((3,)),

time: 40.4 us -> 40.4 us (level)
  the two profiles are of different devices: /device:TPU:8 before, /device:TPU:12 now
where the time goes in v3:
time: 40.4 us; the launch traced here: 40.2 us
  Pallas kernels  39.6 us (98%)
  between operations  0.64 us (2%)
    pallas_call x1, Pallas kernels, body(): pl.pallas_call(functools.partial(exchange_kernel, ring_z, blocks_here, bl...  38.4 us
    pallas_call x1, Pallas kernels, body(): pl.pallas_call(mix_kernel, out_shape=(jax.ShapeDtypeStruct((1, row_count,...  1.15 us

profile of v3, /device:TPU:12, one launch (start us, length us, event | category | flops | bytes accessed | tf_op | source)
XLA Modules:
  0.0 40.2 jit_solution(5229047059309272671)
XLA Ops:
  0.6 38.4 %shard_map.77 = (bf16[320,256]{1,0:T(8,128)(2,1)S(1)}, f32[1,2,320]{2,1,0:T(2,128)S(1)}, bf16[512,1024]{1,0:T(8,128)(2,1)S(1)}, f32[320,1024]{1,0:T(8,128)S(1)}) custom-call(bf16[1,320,2048]{2,1,0:T(8,128)(2,1)} %tokens_hbm.1, bf16[2048,256]{1,0:T(8,128)(2,1)} %wq_hbm.1, bf16[2048,128]{1,0:T(8,128)(2,1)} %wk_hbm.1, bf16[2048,128]{1,0:T(8,128)(2,1)} %wv_hbm.1, ...), custom_call_target="tpu_custom_call" | custom-call | tf_op jit(solution)/shard_map/pallas_call | solution.py:617
  39.1 1.1 %shard_map.78 = (bf16[1,320,1024]{2,1,0:T(8,128)(2,1)}, f32[1,2,320]{2,1,0:T(2,128)}) custom-call(bf16[320,256]{1,0:T(8,128)(2,1)S(1)} %get-tuple-element.6.partner, bf16[512,1024]{1,0:T(8,128)(2,1)S(1)} %get-tuple-element.7.wo, f32[320,1024]{1,0:T(8,128)S(1)} %get-tuple-element.8.own_mixed, f32[1,2,320]{2,1,0:T(2,128)S(1)} %get-tuple-element.9.log_in), custom_call_target="tpu_custom_call" | custom-call | tf_op jit(solution)/shard_map/pallas_call | solution.py:664

commit v4 on v3

--- a/solution.py
+++ b/solution.py
@@ -92,7 +92,7 @@
         return [
             pltpu.make_async_copy(tokens_hbm.at[0, :, deep], tok.at[:, deep], part_sem.at[i, 0]),
             pltpu.make_async_copy(wk_hbm.at[deep], wkv.at[deep, k_lanes], part_sem.at[i, 1]),
-            pltpu.make_async_copy(wv_hbm.at[deep], wkv.at[deep, v_lanes], part_sem.at[i, 2]),
+            pltpu.make_async_copy(wv_hbm.at[deep], wkv.at[deep, v_lanes], part_sem.at[i, 1]),
         ]
 
     load_chosen = pltpu.make_async_copy(chosen_hbm, chosen, load_sem.at[0])
@@ -112,9 +112,10 @@
 
         @pl.loop(0, DEPTH_PARTS)
         def _(i):
-            for load in loads_of(i):
-                load.wait()
             deep = pl.ds(pl.multiple_of(i * part_depth, part_depth), part_depth)
+            loads_of(i)[0].wait()
+            both = wkv.at[deep]
+            pltpu.make_async_copy(both, both, part_sem.at[i, 1]).wait()
             kv_sum[...] += jnp.dot(tok[:, deep], wkv[deep, :], preferred_element_type=f32)
 
         load_wq.start()
@@ -645,7 +646,7 @@
             vmem((3 * RING_Y, 1, 128), jnp.int32),
             pltpu.SMEM((3 * RING_Y, 1, 128), jnp.int32),
             dma((4,)),
-            dma((DEPTH_PARTS, 3)),
+            dma((DEPTH_PARTS, 2)),
             dma((1,)),
             dma(((ring_z // 2 - 3) * chunks + 1,)),
             dma((1,)),

time: 40.4 us -> 40.3 us (level)
  no operation moved by 1% of the time
where the time goes in v4:
time: 40.3 us; the launch traced here: 40.2 us
  Pallas kernels  39.6 us (98%)
  between operations  0.64 us (2%)
    pallas_call x1, Pallas kernels, body(): pl.pallas_call(functools.partial(exchange_kernel, ring_z, blocks_here, bl...  38.4 us
    pallas_call x1, Pallas kernels, body(): pl.pallas_call(mix_kernel, out_shape=(jax.ShapeDtypeStruct((1, row_count,...  1.15 us

profile of v4, /device:TPU:12, one launch (start us, length us, event | category | flops | bytes accessed | tf_op | source)
XLA Modules:
  0.0 40.2 jit_solution(10424382523911772998)
XLA Ops:
  0.6 38.4 %shard_map.77 = (bf16[320,256]{1,0:T(8,128)(2,1)S(1)}, f32[1,2,320]{2,1,0:T(2,128)S(1)}, bf16[512,1024]{1,0:T(8,128)(2,1)S(1)}, f32[320,1024]{1,0:T(8,128)S(1)}) custom-call(bf16[1,320,2048]{2,1,0:T(8,128)(2,1)} %tokens_hbm.1, bf16[2048,256]{1,0:T(8,128)(2,1)} %wq_hbm.1, bf16[2048,128]{1,0:T(8,128)(2,1)} %wk_hbm.1, bf16[2048,128]{1,0:T(8,128)(2,1)} %wv_hbm.1, ...), custom_call_target="tpu_custom_call" | custom-call | tf_op jit(solution)/shard_map/pallas_call | solution.py:618
  39.0 1.1 %shard_map.78 = (bf16[1,320,1024]{2,1,0:T(8,128)(2,1)}, f32[1,2,320]{2,1,0:T(2,128)}) custom-call(bf16[320,256]{1,0:T(8,128)(2,1)S(1)} %get-tuple-element.6.partner, bf16[512,1024]{1,0:T(8,128)(2,1)S(1)} %get-tuple-element.7.wo, f32[320,1024]{1,0:T(8,128)S(1)} %get-tuple-element.8.own_mixed, f32[1,2,320]{2,1,0:T(2,128)S(1)} %get-tuple-element.9.log_in), custom_call_target="tpu_custom_call" | custom-call | tf_op jit(solution)/shard_map/pallas_call | solution.py:665
